TPU v7x, 256 devices: a 4x2x16 block of a 4x16x16 slice. The times are simulated.
256 devices in a mesh: grp: 2 (over y), fs: 32 (over z, core), tp: 4 (over x).
Axes of the slice: x: 4, y: 2, z: 16, core: 2. Of those that a mesh axis runs over, the one named last changes fastest.
The devices are a block of a 4x16x16 slice.
Arguments:
- tokens: bfloat16 [1536, 2048], P(('grp', 'tp')), parts along dimension 0, may hold values from -6 to 6
- norm_gain: float32 [2048], P('fs'), may hold values from 0.1 to 1.9
- up_trained: float32 [2048, 8192], P('fs', 'tp'), may hold values from -0.125 to 0.125
- down_trained: float32 [2048, 8192], P('fs', 'tp'), may hold values from -0.125 to 0.125
Outputs:
- up_serving: bfloat16 [4096, 8192], P('grp', 'fs'), parts along dimension 0
- down_serving: bfloat16 [4096, 8192], P('grp', 'fs'), parts along dimension 0
- prompt_output: bfloat16 [1536, 2048], P(('grp', 'tp'), 'fs'), parts along dimension 0
There are 2 independent parts, one for each index of `grp`. A program takes and returns all parts, laid end to end along the dimension named above; an argument that names none is the same for every part. Nothing has to cross between parts.
All inputs are finite; a program needn't handle non-finite values.
Results may differ from a plain program's by a relative error of at most 0.0074.
Values may be sent and summed in bfloat16 or wider, within the bound.
No kernel may reach another device: no remote copies, remote signals or barrier semaphores. Data moves between devices by JAX's collectives and lax.ppermute only.
A program may use at most 64 MiB of HBM per device.

v0:
```python
import jax
import jax.numpy as jnp
from jax import lax
from jax.sharding import PartitionSpec as P

epsilon = 1e-06
CORES = 2


def joined_along(parts, dim):
    parts = jnp.moveaxis(parts, 0, dim)
    dims = parts.shape
    return parts.reshape(*dims[:dim], dims[dim] * dims[dim + 1], *dims[dim + 2 :])


def copy_for_each(x, axis):
    devices = lax.axis_size(axis)
    return lax.all_to_all(jnp.broadcast_to(x[None], (devices, *x.shape)), axis, 0, 0, tiled=True)


def collect(x, axis, dim):
    return joined_along(copy_for_each(x, axis), dim)


def packed(x):
    rows, cols = x.shape[-2:]
    wide = cols * 2 // 3
    tail = x[..., wide:]
    tail = jnp.concatenate([tail[..., : rows // 2, :], tail[..., rows // 2 :, :]], axis=-1)
    return jnp.concatenate([x[..., :wide], tail], axis=-2)


def unpacked(x, rows):
    wide = x.shape[-1]
    tail = x[..., rows:, :]
    tail = jnp.concatenate([tail[..., : wide // 2], tail[..., wide // 2 :]], axis=-2)
    return jnp.concatenate([x[..., :rows, :], tail], axis=-1)


def sum_at_owner(x, axis):
    devices = lax.axis_size(axis)
    rows = x.shape[0] // devices
    chips = devices // CORES
    parts = packed(x.reshape(chips, CORES, rows, x.shape[1]))
    core = lax.axis_index(axis) % CORES
    away = lax.dynamic_index_in_dim(parts, 1 - core, 1, keepdims=False)
    kept = lax.dynamic_index_in_dim(parts, core, 1, keepdims=False)
    other = lax.ppermute(away, axis, [(i, i ^ 1) for i in range(devices)])
    both = (kept.astype(jnp.float32) + other.astype(jnp.float32)).astype(jnp.bfloat16)
    same_core = [[z * CORES + c for z in range(chips)] for c in range(CORES)]
    arrived = lax.all_to_all(both, axis, 0, 0, axis_index_groups=same_core, tiled=True)
    return unpacked(arrived.astype(jnp.float32).sum(axis=0), rows)


def local(tokens, norm_gain, up_trained, down_trained):
    shards = lax.axis_size("fs")
    groups = lax.axis_size("tp")
    rows_local = up_trained.shape[0]
    cols_local = up_trained.shape[1]
    folded = (norm_gain[:, None] * up_trained).astype(jnp.bfloat16)
    stacked = jnp.stack([folded, down_trained.astype(jnp.bfloat16)])
    served_width = cols_local * groups // shards
    blocks_here = cols_local // served_width
    quarter_rows = rows_local // groups
    pieces = stacked.reshape(2, groups, quarter_rows, blocks_here, served_width)
    moved = lax.all_to_all(pieces, "tp", split_axis=1, concat_axis=3, tiled=True)
    placed = lax.all_to_all(moved, "fs", split_axis=3, concat_axis=2, tiled=True)
    ordered = placed.reshape(2, shards, quarter_rows, served_width)
    joined = collect(ordered, "tp", 2)
    owned = joined.reshape(2, rows_local * shards, served_width)
    up_serving = owned[0]
    down_serving = owned[1]
    values = tokens.astype(jnp.float32)
    scale = lax.rsqrt(jnp.mean(values * values, axis=1, keepdims=True) + epsilon)
    normed = (values * scale).astype(jnp.bfloat16)
    hidden = jnp.dot(normed, up_serving, preferred_element_type=jnp.float32)
    active = jnp.square(jax.nn.relu(hidden)).astype(jnp.bfloat16)
    partial = lax.dot_general(
        down_serving, active, (((1,), (1,)), ((), ())), preferred_element_type=jnp.float32
    ).astype(jnp.bfloat16)
    prompt_output = sum_at_owner(partial, "fs").T.astype(jnp.bfloat16)
    return (up_serving, down_serving, prompt_output)


def solution(mesh):
    in_specs = (P(("grp", "tp"), None), P("fs"), P("fs", "tp"), P("fs", "tp"))
    out_specs = (P("grp", "fs"), P("grp", "fs"), P(("grp", "tp"), "fs"))
    return jax.shard_map(local, mesh=mesh, in_specs=in_specs, out_specs=out_specs, check_vma=False)
```

profile of v0, /device:TPU:40, one launch (start us, length us, event | category | flops | bytes accessed | tf_op | source)
XLA Modules:
  0.0 141.5 jit_solution(10750599824275625618)
XLA Ops:
  0.6 0.0 copy-start.3
  0.6 1.1 convert_element_type.38
  1.8 0.1 copy.24
  1.8 0.0 copy-done.3
  1.8 0.8 multiply_convert_fusion
  2.6 0.1 copy.23
  2.7 0.1 pad_maximum_fusion
  2.8 13.9 %all_to_all.43 = bf16[2,4,16,8,256]{4,3,2,0,1:T(8,128)(2,1)S(1)} all-to-all(bf16[2,4,16,8,256]{4,3,2,0,1:T(8,128)(2,1)S(1)} %copy.17), channel_id=1, replica_groups=mesh['grp'=2,'fs'=32,'tp'=4] {'tp'}, dimensions={1} | all-to-all | bytes 1048576 | tf_op jit(solution)/shard_map/all_to_all | solution.py:66
  16.7 0.1 copy.28
  16.8 0.3 copy.19
  17.1 57.6 %all_to_all.44 = bf16[2,1,16,32,256]{4,2,0,1,3:T(8,128)(2,1)S(1)} all-to-all(bf16[2,1,16,32,256]{4,2,0,1,3:T(8,128)(2,1)S(1)} %copy.19), channel_id=1, replica_groups=mesh['grp'=2,'fs'=32,'tp'=4] {'fs'}, dimensions={3} | all-to-all | bytes 1048576 | tf_op jit(solution)/shard_map/all_to_all | solution.py:67
  74.7 1.5 %broadcast_in_dim.10 = bf16[4,2,32,16,256]{4,3,2,1,0:T(8,128)(2,1)} broadcast(bf16[2,32,16,256]{3,2,1,0:T(8,128)(2,1)S(1)} %copy.20), dimensions={1,2,3,4} | broadcast | bytes 2621440 | tf_op jit(solution)/shard_map/broadcast_in_dim | solution.py:18
  76.2 0.0 copy-start.2
  76.2 3.8 %all-to-all-start.2 = ((bf16[4,2,32,16,256]{4,3,2,1,0:T(8,128)(2,1)}), bf16[4,2,32,16,256]{4,3,2,1,0:T(8,128)(2,1)S(1)}, u32[]{:S(2)}, u32[]{:S(2)}) async-start(bf16[4,2,32,16,256]{4,3,2,1,0:T(8,128)(2,1)} %broadcast_in_dim.10), calls=%async_computation.2 | async-start | bytes 4194304 | tf_op jit(solution)/shard_map/all_to_all | solution.py:18
  80.1 0.0 copy-done.2
  80.1 0.2 fusion
  80.4 26.4 %all-to-all-done.2 = bf16[4,2,32,16,256]{4,3,2,1,0:T(8,128)(2,1)S(1)} async-done(((bf16[4,2,32,16,256]{4,3,2,1,0:T(8,128)(2,1)}), bf16[4,2,32,16,256]{4,3,2,1,0:T(8,128)(2,1)S(1)}, u32[]{:S(2)}, u32[]{:S(2)}) %all-to-all-start.2) | async-done | bytes 2097184 | tf_op jit(solution)/shard_map/all_to_all | solution.py:18
  106.8 0.3 copy.27
  107.1 0.2 fusion.11
  107.3 0.0 copy-start
  107.3 0.0 copy-start.1
  107.3 2.0 %convolution_convert_fusion = bf16[2048,192]{0,1:T(8,128)(2,1)} fusion(bf16[2048,256]{1,0:T(8,128)(2,1)S(1)} %bitcast.36, bf16[2048,256]{1,0:T(8,128)(2,1)S(1)} %bitcast.38, bf16[192,2048]{1,0:T(8,128)(2,1)S(1)} %copy-done.2, f32[192]{0:T(256)S(1)} %add_rsqrt_fusion), kind=kOutput, calls=%fused_computation | convolution fusion | flops 404373504 | bytes 3670784 | tf_op jit(solution)/shard_map/dot_general | solution.py:78
  109.4 0.0 copy-done
  109.4 0.0 copy-done.1
  109.4 1.4 %copy.22 = bf16[2048,192]{1,0:T(8,128)(2,1)S(1)} copy(bf16[2048,192]{0,1:T(8,128)(2,1)} %convolution_convert_fusion) | data formatting | bytes 1572864 | tf_op jit(solution)/shard_map/convert_element_type | solution.py:80
  110.8 0.1 fusion.12
  110.9 0.1 slice.45
  111.1 0.2 maximum_maximum_fusion
  111.3 0.1 collective-permute-start
  111.5 1.7 %collective-permute-done = bf16[16,96,128]{2,1,0:T(8,128)(2,1)S(1)} collective-permute-done((bf16[16,96,128]{2,1,0:T(8,128)(2,1)S(1)}, bf16[16,96,128]{2,1,0:T(8,128)(2,1)S(1)}, u32[]{:S(2)}, u32[]{:S(2)}) %collective-permute-start) | collective-permute-done | bytes 393248 | tf_op jit(solution)/shard_map/ppermute | solution.py:48
  113.1 0.1 fusion.6
  113.3 27.5 %all_to_all.45 = bf16[16,96,128]{2,1,0:T(8,128)(2,1)S(1)} all-to-all(bf16[16,96,128]{2,1,0:T(8,128)(2,1)S(1)} %fusion.6), channel_id=1, replica_groups={{0,8,16,24,32,40,48,56,64,72,80,88,96,104,112,120},{4,12,20,28,36,44,52..., dimensions={0} | all-to-all | bytes 786432 | tf_op jit(solution)/shard_map/all_to_all | solution.py:51
  140.8 0.1 reduce
  140.8 0.1 fusion.13
  140.9 0.6 maximum_bitcast_fusion
  (5 shorter events, 0.1 us)
Async XLA Ops:
  0.6 1.2 copy-start.3
  76.2 3.9 %copy-start.2 = (bf16[192,2048]{1,0:T(8,128)(2,1)S(1)}, bf16[192,2048]{1,0:T(8,128)(2,1)}, u32[]{:S(2)}) copy-start(bf16[192,2048]{1,0:T(8,128)(2,1)} %param.4) | copy-start | bytes 2359300
  76.2 30.5 %all-to-all-start.2 = ((bf16[4,2,32,16,256]{4,3,2,1,0:T(8,128)(2,1)}), bf16[4,2,32,16,256]{4,3,2,1,0:T(8,128)(2,1)S(1)}, u32[]{:S(2)}, u32[]{:S(2)}) async-start(bf16[4,2,32,16,256]{4,3,2,1,0:T(8,128)(2,1)} %broadcast_in_dim.10), calls=%async_computation.2 | async-start | bytes 4194304 | tf_op jit(solution)/shard_map/all_to_all | solution.py:18
  107.3 2.1 %copy-start = (bf16[1,32,4,16,256]{4,3,2,1,0:T(8,128)(2,1)}, bf16[1,32,4,16,256]{4,3,2,1,0:T(8,128)(2,1)S(1)}, u32[]{:S(2)}) copy-start(bf16[1,32,4,16,256]{4,3,2,1,0:T(8,128)(2,1)S(1)} %get-tuple-element.3) | copy-start | bytes 3145732
  107.3 2.1 %copy-start.1 = (bf16[1,32,4,16,256]{4,3,2,1,0:T(8,128)(2,1)}, bf16[1,32,4,16,256]{4,3,2,1,0:T(8,128)(2,1)S(1)}, u32[]{:S(2)}) copy-start(bf16[1,32,4,16,256]{4,3,2,1,0:T(8,128)(2,1)S(1)} %get-tuple-element.4) | copy-start | bytes 3145732
  111.3 1.8 %collective-permute-start = (bf16[16,96,128]{2,1,0:T(8,128)(2,1)S(1)}, bf16[16,96,128]{2,1,0:T(8,128)(2,1)S(1)}, u32[]{:S(2)}, u32[]{:S(2)}) collective-permute-start(bf16[16,96,128]{2,1,0:T(8,128)(2,1)S(1)} %dynamic-slice_bitcast_fusion), channel_id=1, source_target_pairs={{0,4},{4,0},{8,12},{12,8},{16,20},{20,16},{24,28},{28,24},{32,36},... | collective-permute-start | bytes 1179656 | tf_op jit(solution)/shard_map/ppermute | solution.py:48
where the time goes:
time: 142 us
  blocking collectives  99.1 us (70%)
  waiting for transfers between devices  28.1 us (20%)
  local copies, waits for them, and re-layouts  4.34 us (3%)
  starting transfers between devices  3.97 us (3%)
  other arithmetic  3.16 us (2%)
  matrix products  2.05 us (1%)
    all_to_all x1, blocking collectives, local(): lax.all_to_all(moved, 'fs', split_axis=3, concat_axis=2, tiled=True)  57.6 us
    all_to_all x1, blocking collectives, sum_at_owner(): lax.all_to_all(both, axis, 0, 0, axis_index_groups=same_core, tiled=True)  27.5 us
    all_to_all x1, waiting for transfers between devices, copy_for_each(): lax.all_to_all(jnp.broadcast_to(x[None], (devices, *x.shape)), axis, 0, 0...  26.4 us
    all_to_all x1, blocking collectives, local(): lax.all_to_all(pieces, 'tp', split_axis=1, concat_axis=3, tiled=True)  13.9 us
    all_to_all x1, starting transfers between devices, copy_for_each(): lax.all_to_all(jnp.broadcast_to(x[None], (devices, *x.shape)), axis, 0, 0...  3.83 us
  transfers between devices with their start and end apart: 2, of which 2 were waited for; matrix products, arithmetic and copies ran while one was open for 0% of the time, Pallas kernels for 0%

commit v1 on v0

--- a/solution.py
+++ b/solution.py
@@ -64,7 +64,9 @@
     quarter_rows = rows_local // groups
     pieces = stacked.reshape(2, groups, quarter_rows, blocks_here, served_width)
     moved = lax.all_to_all(pieces, "tp", split_axis=1, concat_axis=3, tiled=True)
-    placed = lax.all_to_all(moved, "fs", split_axis=3, concat_axis=2, tiled=True)
+    placed = jnp.concatenate(
+        lax.all_to_all(jnp.stack(jnp.split(moved, lax.axis_size("fs"), axis=3)), "fs", 0, 0), axis=2
+    )
     ordered = placed.reshape(2, shards, quarter_rows, served_width)
     joined = collect(ordered, "tp", 2)
     owned = joined.reshape(2, rows_local * shards, served_width)

time: 142 us -> 143 us (level)
  no operation moved by 1% of the time
where the time goes in v1:
time: 143 us; the launch traced here: 142 us
  blocking collectives  99.1 us (69%)
  waiting for transfers between devices  28.1 us (20%)
  local copies, waits for them, and re-layouts  5.4 us (4%)
  starting transfers between devices  3.97 us (3%)
  other arithmetic  2.51 us (2%)
  matrix products  2.05 us (1%)
    all_to_all x1, blocking collectives, local(): lax.all_to_all(jnp.stack(jnp.split(moved, lax.axis_size('fs'), axis=3)),...  57.6 us
    all_to_all x1, blocking collectives, sum_at_owner(): lax.all_to_all(both, axis, 0, 0, axis_index_groups=same_core, tiled=True)  27.5 us
    all_to_all x1, waiting for transfers between devices, copy_for_each(): lax.all_to_all(jnp.broadcast_to(x[None], (devices, *x.shape)), axis, 0, 0...  26.4 us
    all_to_all x1, blocking collectives, local(): lax.all_to_all(pieces, 'tp', split_axis=1, concat_axis=3, tiled=True)  13.9 us
    all_to_all x1, starting transfers between devices, copy_for_each(): lax.all_to_all(jnp.broadcast_to(x[None], (devices, *x.shape)), axis, 0, 0...  3.83 us
  transfers between devices with their start and end apart: 2, of which 2 were waited for; matrix products, arithmetic and copies ran while one was open for 0% of the time, Pallas kernels for 0%

profile of v1, /device:TPU:40, one launch (start us, length us, event | category | flops | bytes accessed | tf_op | source)
XLA Modules:
  0.0 142.2 jit_solution(573584219087924942)
XLA Ops:
  0.6 0.0 copy-start.3
  0.6 1.2 multiply_convert_fusion
  1.8 0.1 copy.664
  1.9 0.0 copy-done.3
  2.0 0.1 copy.665
  2.0 0.1 pad_maximum_fusion
  2.1 13.9 %all_to_all.33 = bf16[2,4,16,8,256]{4,3,2,0,1:T(8,128)(2,1)S(1)} all-to-all(bf16[2,4,16,8,256]{4,3,2,0,1:T(8,128)(2,1)S(1)} %copy.625), channel_id=1, replica_groups=mesh['grp'=2,'fs'=32,'tp'=4] {'tp'}, dimensions={1} | all-to-all | bytes 1048576 | tf_op jit(solution)/shard_map/all_to_all | solution.py:66
  16.0 0.1 copy_bitcast_fusion
  16.1 0.5 fusion.14
  16.6 0.7 fusion.13
  17.8 57.6 %all_to_all.34 = bf16[32,2,1,16,1,256]{5,3,1,4,2,0:T(8,128)(2,1)S(1)} all-to-all(bf16[32,2,1,16,1,256]{5,3,1,4,2,0:T(8,128)(2,1)S(1)} %constant_dynamic-update-slice_fusion), channel_id=1, replica_groups=mesh['grp'=2,'fs'=32,'tp'=4] {'fs'}, dimensions={0} | all-to-all | bytes 1048576 | tf_op jit(solution)/shard_map/all_to_all | solution.py:68
  75.4 1.5 %broadcast_in_dim.10 = bf16[4,2,32,16,256]{4,3,2,1,0:T(8,128)(2,1)} broadcast(bf16[2,32,16,256]{3,2,1,0:T(8,128)(2,1)S(1)} %copy.628), dimensions={1,2,3,4} | broadcast | bytes 2621440 | tf_op jit(solution)/shard_map/broadcast_in_dim | solution.py:18
  77.0 0.0 copy-start.2
  77.0 3.8 %all-to-all-start.2 = ((bf16[4,2,32,16,256]{4,3,2,1,0:T(8,128)(2,1)}), bf16[4,2,32,16,256]{4,3,2,1,0:T(8,128)(2,1)S(1)}, u32[]{:S(2)}, u32[]{:S(2)}) async-start(bf16[4,2,32,16,256]{4,3,2,1,0:T(8,128)(2,1)} %broadcast_in_dim.10), calls=%async_computation.2 | async-start | bytes 4194304 | tf_op jit(solution)/shard_map/all_to_all | solution.py:18
  80.8 0.0 copy-done.2
  80.8 0.2 fusion
  81.1 26.4 %all-to-all-done.2 = bf16[4,2,32,16,256]{4,3,2,1,0:T(8,128)(2,1)S(1)} async-done(((bf16[4,2,32,16,256]{4,3,2,1,0:T(8,128)(2,1)}), bf16[4,2,32,16,256]{4,3,2,1,0:T(8,128)(2,1)S(1)}, u32[]{:S(2)}, u32[]{:S(2)}) %all-to-all-start.2) | async-done | bytes 2097184 | tf_op jit(solution)/shard_map/all_to_all | solution.py:18
  107.5 0.2 fusion.11
  107.7 0.1 copy.629
  107.9 0.0 copy-start
  107.9 0.1 copy.630
  108.0 0.0 copy-start.1
  108.0 2.1 %convolution_convert_fusion = bf16[2048,192]{0,1:T(8,128)(2,1)} fusion(bf16[2048,256]{1,0:T(8,128)(2,1)S(1)} %bitcast.98, bf16[2048,256]{1,0:T(8,128)(2,1)S(1)} %bitcast.96, bf16[192,2048]{1,0:T(8,128)(2,1)S(1)} %copy-done.2, f32[192]{0:T(256)S(1)} %add_rsqrt_fusion), kind=kOutput, calls=%fused_computation | convolution fusion | flops 404373504 | bytes 3670784 | tf_op jit(solution)/shard_map/dot_general | solution.py:80
  110.1 0.0 copy-done
  110.1 0.0 copy-done.1
  110.1 1.4 %copy.631 = bf16[2048,192]{1,0:T(8,128)(2,1)S(1)} copy(bf16[2048,192]{0,1:T(8,128)(2,1)} %convolution_convert_fusion) | data formatting | bytes 1572864 | tf_op jit(solution)/shard_map/convert_element_type | solution.py:82
  111.5 0.1 fusion.12
  111.6 0.1 slice.45
  111.7 0.2 maximum_maximum_fusion
  112.0 0.1 collective-permute-start
  112.1 1.7 %collective-permute-done = bf16[16,96,128]{2,1,0:T(8,128)(2,1)S(1)} collective-permute-done((bf16[16,96,128]{2,1,0:T(8,128)(2,1)S(1)}, bf16[16,96,128]{2,1,0:T(8,128)(2,1)S(1)}, u32[]{:S(2)}, u32[]{:S(2)}) %collective-permute-start) | collective-permute-done | bytes 393248 | tf_op jit(solution)/shard_map/ppermute | solution.py:48
  113.8 0.1 fusion.6
  113.9 27.5 %all_to_all.35 = bf16[16,96,128]{2,1,0:T(8,128)(2,1)S(1)} all-to-all(bf16[16,96,128]{2,1,0:T(8,128)(2,1)S(1)} %fusion.6), channel_id=1, replica_groups={{0,8,16,24,32,40,48,56,64,72,80,88,96,104,112,120},{4,12,20,28,36,44,52..., dimensions={0} | all-to-all | bytes 786432 | tf_op jit(solution)/shard_map/all_to_all | solution.py:51
  141.4 0.1 reduce
  141.5 0.1 fusion.15
  141.6 0.6 maximum_bitcast_fusion
  (38 shorter events, 0.4 us)
Async XLA Ops:
  0.6 1.3 copy-start.3
  77.0 3.9 %copy-start.2 = (bf16[192,2048]{1,0:T(8,128)(2,1)S(1)}, bf16[192,2048]{1,0:T(8,128)(2,1)}, u32[]{:S(2)}) copy-start(bf16[192,2048]{1,0:T(8,128)(2,1)} %param.4) | copy-start | bytes 2359300
  77.0 30.5 %all-to-all-start.2 = ((bf16[4,2,32,16,256]{4,3,2,1,0:T(8,128)(2,1)}), bf16[4,2,32,16,256]{4,3,2,1,0:T(8,128)(2,1)S(1)}, u32[]{:S(2)}, u32[]{:S(2)}) async-start(bf16[4,2,32,16,256]{4,3,2,1,0:T(8,128)(2,1)} %broadcast_in_dim.10), calls=%async_computation.2 | async-start | bytes 4194304 | tf_op jit(solution)/shard_map/all_to_all | solution.py:18
  107.9 2.2 %copy-start = (bf16[1,32,4,16,256]{4,3,2,1,0:T(8,128)(2,1)}, bf16[1,32,4,16,256]{4,3,2,1,0:T(8,128)(2,1)S(1)}, u32[]{:S(2)}) copy-start(bf16[1,32,4,16,256]{4,3,2,1,0:T(8,128)(2,1)S(1)} %copy.629) | copy-start | bytes 3145732
  108.0 2.1 %copy-start.1 = (bf16[1,32,4,16,256]{4,3,2,1,0:T(8,128)(2,1)}, bf16[1,32,4,16,256]{4,3,2,1,0:T(8,128)(2,1)S(1)}, u32[]{:S(2)}) copy-start(bf16[1,32,4,16,256]{4,3,2,1,0:T(8,128)(2,1)S(1)} %copy.630) | copy-start | bytes 3145732
  112.0 1.8 %collective-permute-start = (bf16[16,96,128]{2,1,0:T(8,128)(2,1)S(1)}, bf16[16,96,128]{2,1,0:T(8,128)(2,1)S(1)}, u32[]{:S(2)}, u32[]{:S(2)}) collective-permute-start(bf16[16,96,128]{2,1,0:T(8,128)(2,1)S(1)} %dynamic-slice_bitcast_fusion), channel_id=1, source_target_pairs={{0,4},{4,0},{8,12},{12,8},{16,20},{20,16},{24,28},{28,24},{32,36},... | collective-permute-start | bytes 1179656 | tf_op jit(solution)/shard_map/ppermute | solution.py:48
